TPU v7x, 512 devices: a whole 4x8x8 slice. The times are simulated.
512 devices in a mesh: ep: 32 (over z, x), tp: 16 (over y, core).
Axes of the slice: x: 4, y: 8, z: 8, core: 2. Of those that a mesh axis runs over, the one named last changes fastest.
Arguments:
- tokens: bfloat16 [256, 4096], P('ep', 'tp'), may hold values from -6 to 6
- norm_gain: float32 [4096], replicated, may hold values from 0.1 to 1.9
- route_experts: int32 [256, 2], P('ep'), may hold values from 0 to 63, all different within a row; in each aligned block of 8 rows (0 to 7, 8 to 15, ...) at most 2 rows name the same one
- route_logits: float32 [256, 2], P('ep'), may hold values from -4 to 4
- expert_gate: bfloat16 [64, 4096, 1024], P('ep', None, 'tp'), may hold values from -0.09375 to 0.09375
- expert_up: bfloat16 [64, 4096, 1024], P('ep', None, 'tp'), may hold values from -0.09375 to 0.09375
- expert_down: bfloat16 [64, 1024, 4096], P('ep', 'tp'), may hold values from -0.1875 to 0.1875
- dense_gate: bfloat16 [4096, 1024], P(None, 'tp'), may hold values from -0.09375 to 0.09375
- dense_up: bfloat16 [4096, 1024], P(None, 'tp'), may hold values from -0.09375 to 0.09375
- dense_down: bfloat16 [1024, 4096], P('tp'), may hold values from -0.1875 to 0.1875
- mix_weight: float32 [4096], replicated, may hold values from -0.09375 to 0.09375
- out_gain: float32 [4096], P('tp'), may hold values from 0.1 to 1.9
Outputs:
- result: bfloat16 [256, 4096], P('ep', 'tp')
Inputs may be any that keep to these rules, and one draw needn't show every extreme that they name: `route_experts`: each row names 2 different experts; the 8 rows of one index of ep (aligned blocks) name any one expert at most 2 times, and some block names some expert exactly 2 times; every expert is named somewhere.
All inputs are finite; a program needn't handle non-finite values.
Results may differ from a plain program's by a relative error of at most 0.0025.
Values may be sent and summed in bfloat16 or wider, within the bound.
A program may use at most 64 MiB of HBM per device.

v0:
```python
import jax
import jax.numpy as jnp
from jax import lax
from jax.sharding import Mesh
from jax.sharding import PartitionSpec as P

CAP = 2
TP = ("tp_0", "tp_1")
norm_eps = 1e-06


def summed_rows(x, axes, dim):
    if not axes:
        return x
    nearer = lax.psum_scatter(x, axes[0], scatter_dimension=dim, tiled=True)
    return summed_rows(nearer, axes[1:], dim)


def local(
    tokens,
    norm_gain,
    route_experts,
    route_logits,
    expert_gate,
    expert_up,
    expert_down,
    dense_gate,
    dense_up,
    dense_down,
    mix_weight,
    out_gain,
):
    tok_rows, width_part = tokens.shape
    groups = lax.axis_size(TP)
    width = width_part * groups
    whole_rows = lax.all_gather(tokens, TP, axis=1, tiled=True).astype(jnp.float32)
    normed = (
        whole_rows
        * lax.rsqrt(jnp.mean(whole_rows * whole_rows, axis=1, keepdims=True) + norm_eps)
        * norm_gain
    ).astype(jnp.bfloat16)
    weights = jax.nn.softmax(route_logits, axis=-1)
    top_count = route_experts.shape[1]
    local_experts = expert_gate.shape[0]
    peer_count = lax.axis_size("ep")
    experts = local_experts * peer_count
    dense_hidden = (
        jax.nn.silu(jnp.dot(normed, dense_gate, preferred_element_type=jnp.float32))
        * jnp.dot(normed, dense_up, preferred_element_type=jnp.float32)
    ).astype(jnp.bfloat16)
    dense_out = summed_rows(
        jnp.dot(dense_hidden, dense_down, preferred_element_type=jnp.float32), TP, 1
    )
    mix_gate = jax.nn.sigmoid(
        jnp.dot(normed.astype(jnp.float32), mix_weight, precision=lax.Precision.HIGHEST)
    )
    flat_routes = route_experts.reshape(-1)
    expert_ids = jnp.arange(experts, dtype=jnp.int32)
    capacity = CAP
    slot_count = experts * capacity
    route_hits = (flat_routes[:, None] == expert_ids[None, :]).astype(jnp.int32)
    before = jnp.cumsum(route_hits, axis=0) - route_hits
    slot_rank = jnp.sum(before * route_hits, axis=1)
    position = flat_routes * capacity + slot_rank
    onehot_place = (position[:, None] == jnp.arange(slot_count, dtype=jnp.int32)[None, :]).astype(
        jnp.float32
    )
    placing = jnp.sum(onehot_place.reshape(tok_rows, top_count, slot_count), axis=1).T.astype(
        jnp.bfloat16
    )
    outgoing = jnp.dot(placing, normed, preferred_element_type=jnp.float32).astype(jnp.bfloat16)
    received = lax.all_to_all(outgoing, "ep", split_axis=0, concat_axis=0, tiled=True)
    arranged = (
        received.reshape(peer_count, local_experts, capacity, width)
        .transpose(1, 0, 2, 3)
        .reshape(local_experts, peer_count * capacity, width)
    )
    gate_act = jnp.einsum("erd,edf->erf", arranged, expert_gate, preferred_element_type=jnp.float32)
    up_act = jnp.einsum("erd,edf->erf", arranged, expert_up, preferred_element_type=jnp.float32)
    hidden = (jax.nn.silu(gate_act) * up_act).astype(jnp.bfloat16)
    partial_value = jnp.einsum(
        "erf,efd->erd", hidden, expert_down, preferred_element_type=jnp.float32
    )
    summed = lax.psum_scatter(partial_value, TP, scatter_dimension=2, tiled=True)
    back_send = (
        summed.reshape(local_experts, peer_count, capacity, width_part)
        .transpose(1, 0, 2, 3)
        .reshape(slot_count, width_part)
    )
    returned = lax.all_to_all(back_send, "ep", split_axis=0, concat_axis=0, tiled=True)
    combine_map = jnp.sum(
        (onehot_place * weights.reshape(-1)[:, None]).reshape(tok_rows, top_count, slot_count),
        axis=1,
    )
    expert_mix = jnp.dot(combine_map, returned, precision=lax.Precision.HIGHEST)
    combined = expert_mix + mix_gate[:, None] * dense_out
    squares_out = lax.psum(jnp.sum(combined * combined, axis=1), TP)
    result = combined * lax.rsqrt(squares_out[:, None] / width + norm_eps) * out_gain
    return result.astype(jnp.bfloat16)


def solution(mesh):
    split = Mesh(mesh.devices.reshape(mesh.shape["ep"], 8, 2), ("ep", "tp_0", "tp_1"))
    in_specs = (
        P("ep", TP),
        P(),
        P("ep", None),
        P("ep", None),
        P("ep", None, TP),
        P("ep", None, TP),
        P("ep", TP, None),
        P(None, TP),
        P(None, TP),
        P(TP, None),
        P(),
        P(TP),
    )
    out_specs = P("ep", TP)
    return jax.shard_map(local, mesh=split, in_specs=in_specs, out_specs=out_specs, check_vma=False)
```

profile of v0, /device:TPU:2, one launch (start us, length us, event | category | flops | bytes accessed | tf_op | source)
XLA Modules:
  0.0 229.2 jit_solution(5264460515615627035)
XLA Ops:
  6.5 0.0 copy-start
  6.5 0.0 reduce-scatter.4.cloned.1.call-start
  6.5 0.8 reduce_max.9
  7.3 0.7 fusion.26
  8.0 0.7 fusion.25
  8.7 0.8 copy.34
  9.5 0.1 eq.30
  9.6 0.1 fusion.17
  9.7 0.2 select_reduce_fusion.1
  9.8 0.1 reduce_sum.57
  9.9 0.1 copy.36
  10.0 18.0 %all_gather.3 = bf16[8,4096]{1,0:T(8,128)(2,1)S(1)} all-gather(bf16[8,256]{1,0:T(8,128)(2,1)} %param.12), channel_id=1, replica_groups=mesh['ep'=32,'tp_0'=8,'tp_1'=2] {'tp_0','tp_1'}, dimensions={1}, use_global_device_ids=true | all-gather | bytes 69632 | tf_op jit(solution)/shard_map/all_gather | solution.py:36
  28.0 0.1 fusion.8
  28.2 0.1 convert_reduce_fusion
  28.2 1.2 convolution_convert_fusion
  29.5 0.4 all_to_all.14
  29.9 41.8 %all_to_all.21 = bf16[32,4,4096]{2,1,0:T(4,128)(2,1)S(1)} all-to-all(bf16[32,4,4096]{2,1,0:T(4,128)(2,1)S(1)} %all_to_all.14), channel_id=1, replica_groups=mesh['ep'=32,'tp_0'=8,'tp_1'=2] {'ep'}, dimensions={0} | all-to-all | bytes 2097152 | tf_op jit(solution)/shard_map/all_to_all | solution.py:72
  71.7 0.5 reshape.67
  72.3 2.0 copy.41
  74.3 0.0 copy-start.1
  74.3 1.6 reshape.68
  75.9 0.0 copy-done.1
  75.9 0.4 fusion.35
  76.3 0.0 copy-done
  76.3 3.4 %fusion.1 = f32[2,64,4096]{2,1,0:T(8,128)} fusion(bf16[2,64,4096]{2,1,0:T(8,128)(2,1)S(1)} %copy-done, bf16[2,64,4096]{2,1,0:T(8,128)(2,1)S(1)} %reshape.68, bf16[2,4096,64]{1,2,0:T(8,128)(2,1)} %param.17, f32[2,64,64]{2,1,0:T(8,128)S(1)} %fusion.35), kind=kOutput, calls=%fused_computation.3 | convolution fusion | flops 134266880 | bytes 5275648 | tf_op jit(solution)/shard_map/erf,efd->erd/dot_general | solution.py:81
  79.7 0.0 copy-start.2
  79.7 0.0 copy-start.5
  79.7 0.0 copy-start.3
  79.7 0.0 copy-start.4
  79.7 0.0 copy-start.7
  79.7 0.0 reduce-scatter.4.cloned.1.call-update
  79.7 0.0 copy-start.6
  79.8 0.0 reduce-scatter.6.cloned.1.call-start
  79.8 0.9 copy-done.2
  80.7 0.0 copy-done.5
  80.7 0.3 fusion.31
  81.0 0.0 copy-done.3
  81.0 0.0 copy-done.4
  81.1 1.3 fusion.3
  82.3 0.0 reduce-scatter.6.cloned.1.call-update
  82.4 53.8 %reduce-scatter.4.cloned.1.call-done = f32[2,64,256]{2,1,0:T(8,128)} async-done(((f32[2,64,4096]{2,1,0:T(8,128)}), f32[2,64,256]{2,1,0:T(8,128)}) %reduce-scatter.4.cloned.1.call-update) | async-done | bytes 131088 | tf_op jit(solution)/shard_map/reduce_scatter | solution.py:84
  136.1 1.0 reshape.69
  137.1 0.7 copy.39
  137.8 10.5 %all-to-all-start.1 = ((f32[32,4,256]{2,1,0:T(4,128)}), f32[32,4,256]{2,1,0:T(4,128)S(1)}, u32[]{:S(2)}, u32[]{:S(2)}) async-start(f32[32,4,256]{2,1,0:T(4,128)} %copy.39), calls=%async_computation.2 | async-start | bytes 262144 | tf_op jit(solution)/shard_map/all_to_all | solution.py:90
  148.3 0.0 reduce-scatter.8.cloned.1.call-start
  148.4 28.9 %reduce-scatter.6.cloned.1.call-done = f32[8,512]{1,0:T(8,128)} async-done(((f32[8,4096]{1,0:T(8,128)}), f32[8,512]{1,0:T(8,128)}) %reduce-scatter.6.cloned.1.call-update) | async-done | bytes 16400 | tf_op jit(solution)/shard_map/reduce_scatter | solution.py:15
  177.3 0.0 reduce-scatter.8.cloned.1.call-update
  177.3 0.0 copy-done.7
  177.3 0.3 fusion.7
  177.6 0.0 all-to-all-done.1
  177.7 0.1 all_to_all.18
  177.7 16.9 %reduce-scatter.8.cloned.1.call-done = f32[8,256]{1,0:T(8,128)} async-done(((f32[8,512]{1,0:T(8,128)}), f32[8,256]{1,0:T(8,128)}) %reduce-scatter.8.cloned.1.call-update) | async-done | bytes 8208 | tf_op jit(solution)/shard_map/reduce_scatter | solution.py:15
  194.6 1.0 multiply_reduce_fusion
  195.6 26.3 %psum.7 = f32[8]{0:T(128)S(1)} all-reduce(f32[8]{0:T(128)S(1)} %get-tuple-element.7), channel_id=1, replica_groups=mesh['ep'=32,'tp_0'=8,'tp_1'=2] {'tp_0','tp_1'}, use_global_device_ids=true, to_apply=%region_11.12 | all-reduce | flops 8 | bytes 64 | tf_op jit(solution)/shard_map/psum | solution.py:97
  222.0 0.0 copy-done.6
  222.0 0.7 multiply_convert_fusion
  (5 shorter events, 0.1 us)
Async XLA Ops:
  6.5 69.8 %copy-start = (bf16[2,64,4096]{2,1,0:T(8,128)(2,1)S(1)}, bf16[2,64,4096]{2,1,0:T(8,128)(2,1)}, u32[]{:S(2)}) copy-start(bf16[2,64,4096]{2,1,0:T(8,128)(2,1)} %param.18) | copy-start | bytes 3145732
  6.5 129.6 %reduce-scatter.4.cloned.1.call-start = ((), (), s32[]{:S(2)}) async-start(), calls=%async_computation.5 | async-start | bytes 2228224 | tf_op jit(solution)/shard_map/reduce_scatter | solution.py:84
  74.3 1.6 copy-start.1
  79.7 1.0 copy-start.2
  79.7 1.0 copy-start.5
  79.7 1.3 copy-start.3
  79.7 1.4 copy-start.4
  79.7 97.6 %copy-start.7 = (f32[4096]{0:T(1024)S(1)}, f32[4096]{0:T(1024)}, u32[]{:S(2)}) copy-start(f32[4096]{0:T(1024)} %param.22) | copy-start | bytes 49156
  79.7 142.2 %copy-start.6 = (f32[256]{0:T(256)S(1)}, f32[256]{0:T(256)}, u32[]{:S(2)}) copy-start(f32[256]{0:T(256)} %param.23) | copy-start | bytes 3076
  79.8 97.6 %reduce-scatter.6.cloned.1.call-start = ((), (), s32[]{:S(2)}) async-start(), calls=%async_computation.6 | async-start | bytes 147456 | tf_op jit(solution)/shard_map/reduce_scatter | solution.py:15
  137.8 39.8 %all-to-all-start.1 = ((f32[32,4,256]{2,1,0:T(4,128)}), f32[32,4,256]{2,1,0:T(4,128)S(1)}, u32[]{:S(2)}, u32[]{:S(2)}) async-start(f32[32,4,256]{2,1,0:T(4,128)} %copy.39), calls=%async_computation.2 | async-start | bytes 262144 | tf_op jit(solution)/shard_map/all_to_all | solution.py:90
  148.3 46.3 %reduce-scatter.8.cloned.1.call-start = ((), (), s32[]{:S(2)}) async-start(), calls=%async_computation.7 | async-start | bytes 24576 | tf_op jit(solution)/shard_map/reduce_scatter | solution.py:15
Sparse Core Ops, SparseCore 0:
  79.9 56.2 reduce-scatter.3
  138.9 38.3 reduce-scatter.5
  180.0 14.5 reduce-scatter.7
where the time goes:
time: 230 us; the launch traced here: 229 us
  waiting for transfers between devices  99.7 us (43%)
  blocking collectives  86.2 us (37%)
  between operations  13.2 us (6%)
  starting transfers between devices  10.6 us (5%)
  local copies, waits for them, and re-layouts  8.3 us (4%)
  matrix products  7.8 us (3%)
  other arithmetic  3.38 us (1%)
    reduce_scatter x1, waiting for transfers between devices, local(): lax.psum_scatter(partial_value, TP, scatter_dimension=2, tiled=True)  53.8 us
    reduce_scatter x2, waiting for transfers between devices, summed_rows(): nearer = lax.psum_scatter(x, axes[0], scatter_dimension=dim, tiled=True)  45.8 us
    all_to_all x1, blocking collectives, local(): lax.all_to_all(outgoing, 'ep', split_axis=0, concat_axis=0, tiled=True)  41.8 us
    psum x1, blocking collectives, local(): squares_out = lax.psum(jnp.sum(combined * combined, axis=1), TP)  26.3 us
    all_gather x1, blocking collectives, local(): lax.all_gather(tokens, TP, axis=1, tiled=True).astype(jnp.float32)  18 us
    all_to_all x1, starting transfers between devices, local(): lax.all_to_all(back_send, 'ep', split_axis=0, concat_axis=0, tiled=True)  10.5 us
  transfers between devices with their start and end apart: 4, of which 3 were waited for; matrix products, arithmetic and copies ran while one was open for 2% of the time, Pallas kernels for 0%

commit v1 on v0

--- a/solution.py
+++ b/solution.py
@@ -94,7 +94,9 @@
     )
     expert_mix = jnp.dot(combine_map, returned, precision=lax.Precision.HIGHEST)
     combined = expert_mix + mix_gate[:, None] * dense_out
-    squares_out = lax.psum(jnp.sum(combined * combined, axis=1), TP)
+    squares_out = jnp.sum(combined * combined, axis=1)
+    for name in ("tp_1", "tp_0"):
+        squares_out = lax.psum(squares_out, name)
     result = combined * lax.rsqrt(squares_out[:, None] / width + norm_eps) * out_gain
     return result.astype(jnp.bfloat16)
 

time: 230 us -> 223 us (0.970)
  blocking collectives: 86.2 us -> 79.3 us
    psum x1 -> x2, blocking collectives: 26.3 us -> 19.5 us  [local(): squares_out = lax.psum(squares_out, name)]
where the time goes in v1:
time: 223 us; the launch traced here: 222 us
  waiting for transfers between devices  99.7 us (45%)
  blocking collectives  79.3 us (36%)
  between operations  13.2 us (6%)
  starting transfers between devices  10.6 us (5%)
  local copies, waits for them, and re-layouts  8.3 us (4%)
  matrix products  7.8 us (3%)
  other arithmetic  3.38 us (2%)
    reduce_scatter x1, waiting for transfers between devices, local(): lax.psum_scatter(partial_value, TP, scatter_dimension=2, tiled=True)  53.8 us
    reduce_scatter x2, waiting for transfers between devices, summed_rows(): nearer = lax.psum_scatter(x, axes[0], scatter_dimension=dim, tiled=True)  45.8 us
    all_to_all x1, blocking collectives, local(): lax.all_to_all(outgoing, 'ep', split_axis=0, concat_axis=0, tiled=True)  41.8 us
    psum x2, blocking collectives, local(): squares_out = lax.psum(squares_out, name)  19.5 us
    all_gather x1, blocking collectives, local(): lax.all_gather(tokens, TP, axis=1, tiled=True).astype(jnp.float32)  18 us
    all_to_all x1, starting transfers between devices, local(): lax.all_to_all(back_send, 'ep', split_axis=0, concat_axis=0, tiled=True)  10.5 us
  transfers between devices with their start and end apart: 4, of which 3 were waited for; matrix products, arithmetic and copies ran while one was open for 2% of the time, Pallas kernels for 0%

profile of v1, /device:TPU:2, one launch (start us, length us, event | category | flops | bytes accessed | tf_op | source)
XLA Modules:
  0.0 222.3 jit_solution(1609646129384233663)
XLA Ops:
  6.5 0.0 copy-start
  6.5 0.0 reduce-scatter.4.cloned.1.call-start
  6.5 0.8 reduce_max.9
  7.3 0.7 fusion.26
  8.0 0.7 fusion.25
  8.7 0.8 copy.34
  9.5 0.1 eq.30
  9.6 0.1 fusion.17
  9.7 0.2 select_reduce_fusion.1
  9.8 0.1 reduce_sum.57
  9.9 0.1 copy.36
  10.0 18.0 %all_gather.3 = bf16[8,4096]{1,0:T(8,128)(2,1)S(1)} all-gather(bf16[8,256]{1,0:T(8,128)(2,1)} %param.12), channel_id=1, replica_groups=mesh['ep'=32,'tp_0'=8,'tp_1'=2] {'tp_0','tp_1'}, dimensions={1}, use_global_device_ids=true | all-gather | bytes 69632 | tf_op jit(solution)/shard_map/all_gather | solution.py:36
  28.0 0.1 fusion.8
  28.2 0.1 convert_reduce_fusion
  28.2 1.2 convolution_convert_fusion
  29.5 0.4 all_to_all.14
  29.9 41.8 %all_to_all.21 = bf16[32,4,4096]{2,1,0:T(4,128)(2,1)S(1)} all-to-all(bf16[32,4,4096]{2,1,0:T(4,128)(2,1)S(1)} %all_to_all.14), channel_id=1, replica_groups=mesh['ep'=32,'tp_0'=8,'tp_1'=2] {'ep'}, dimensions={0} | all-to-all | bytes 2097152 | tf_op jit(solution)/shard_map/all_to_all | solution.py:72
  71.7 0.5 reshape.67
  72.3 2.0 copy.41
  74.3 0.0 copy-start.1
  74.3 1.6 reshape.68
  75.9 0.0 copy-done.1
  75.9 0.4 fusion.35
  76.3 0.0 copy-done
  76.3 3.4 %fusion.1 = f32[2,64,4096]{2,1,0:T(8,128)} fusion(bf16[2,64,4096]{2,1,0:T(8,128)(2,1)S(1)} %copy-done, bf16[2,64,4096]{2,1,0:T(8,128)(2,1)S(1)} %reshape.68, bf16[2,4096,64]{1,2,0:T(8,128)(2,1)} %param.17, f32[2,64,64]{2,1,0:T(8,128)S(1)} %fusion.35), kind=kOutput, calls=%fused_computation.3 | convolution fusion | flops 134266880 | bytes 5275648 | tf_op jit(solution)/shard_map/erf,efd->erd/dot_general | solution.py:81
  79.7 0.0 copy-start.2
  79.7 0.0 copy-start.5
  79.7 0.0 copy-start.3
  79.7 0.0 copy-start.4
  79.7 0.0 copy-start.7
  79.7 0.0 reduce-scatter.4.cloned.1.call-update
  79.7 0.0 copy-start.6
  79.8 0.0 reduce-scatter.6.cloned.1.call-start
  79.8 0.9 copy-done.2
  80.7 0.0 copy-done.5
  80.7 0.3 fusion.31
  81.0 0.0 copy-done.3
  81.0 0.0 copy-done.4
  81.1 1.3 fusion.3
  82.3 0.0 reduce-scatter.6.cloned.1.call-update
  82.4 53.8 %reduce-scatter.4.cloned.1.call-done = f32[2,64,256]{2,1,0:T(8,128)} async-done(((f32[2,64,4096]{2,1,0:T(8,128)}), f32[2,64,256]{2,1,0:T(8,128)}) %reduce-scatter.4.cloned.1.call-update) | async-done | bytes 131088 | tf_op jit(solution)/shard_map/reduce_scatter | solution.py:84
  136.1 1.0 reshape.69
  137.1 0.7 copy.39
  137.8 10.5 %all-to-all-start.1 = ((f32[32,4,256]{2,1,0:T(4,128)}), f32[32,4,256]{2,1,0:T(4,128)S(1)}, u32[]{:S(2)}, u32[]{:S(2)}) async-start(f32[32,4,256]{2,1,0:T(4,128)} %copy.39), calls=%async_computation.2 | async-start | bytes 262144 | tf_op jit(solution)/shard_map/all_to_all | solution.py:90
  148.3 0.0 reduce-scatter.8.cloned.1.call-start
  148.4 28.9 %reduce-scatter.6.cloned.1.call-done = f32[8,512]{1,0:T(8,128)} async-done(((f32[8,4096]{1,0:T(8,128)}), f32[8,512]{1,0:T(8,128)}) %reduce-scatter.6.cloned.1.call-update) | async-done | bytes 16400 | tf_op jit(solution)/shard_map/reduce_scatter | solution.py:15
  177.3 0.0 reduce-scatter.8.cloned.1.call-update
  177.3 0.0 copy-done.7
  177.3 0.3 fusion.7
  177.6 0.0 all-to-all-done.1
  177.7 0.1 all_to_all.18
  177.7 16.9 %reduce-scatter.8.cloned.1.call-done = f32[8,256]{1,0:T(8,128)} async-done(((f32[8,512]{1,0:T(8,128)}), f32[8,256]{1,0:T(8,128)}) %reduce-scatter.8.cloned.1.call-update) | async-done | bytes 8208 | tf_op jit(solution)/shard_map/reduce_scatter | solution.py:15
  194.6 1.0 multiply_reduce_fusion
  195.6 2.5 %psum.14 = f32[8]{0:T(128)S(1)} all-reduce(f32[8]{0:T(128)S(1)} %get-tuple-element.7), channel_id=1, replica_groups=mesh['ep'=32,'tp_0'=8,'tp_1'=2] {'tp_1'}, use_global_device_ids=true, to_apply=%region_11.12 | all-reduce | flops 8 | bytes 64 | tf_op jit(solution)/shard_map/psum | solution.py:99
  198.1 17.0 %psum.15 = f32[8]{0:T(128)S(1)} all-reduce(f32[8]{0:T(128)S(1)} %psum.14), channel_id=1, replica_groups=mesh['ep'=32,'tp_0'=8,'tp_1'=2] {'tp_0'}, use_global_device_ids=true, to_apply=%region_12.13 | all-reduce | flops 8 | bytes 64 | tf_op jit(solution)/shard_map/psum | solution.py:99
  215.1 0.0 copy-done.6
  215.1 0.7 multiply_convert_fusion
  (5 shorter events, 0.1 us)
Async XLA Ops:
  6.5 69.8 %copy-start = (bf16[2,64,4096]{2,1,0:T(8,128)(2,1)S(1)}, bf16[2,64,4096]{2,1,0:T(8,128)(2,1)}, u32[]{:S(2)}) copy-start(bf16[2,64,4096]{2,1,0:T(8,128)(2,1)} %param.18) | copy-start | bytes 3145732
  6.5 129.6 %reduce-scatter.4.cloned.1.call-start = ((), (), s32[]{:S(2)}) async-start(), calls=%async_computation.5 | async-start | bytes 2228224 | tf_op jit(solution)/shard_map/reduce_scatter | solution.py:84
  74.3 1.6 copy-start.1
  79.7 1.0 copy-start.2
  79.7 1.0 copy-start.5
  79.7 1.3 copy-start.3
  79.7 1.4 copy-start.4
  79.7 97.6 %copy-start.7 = (f32[4096]{0:T(1024)S(1)}, f32[4096]{0:T(1024)}, u32[]{:S(2)}) copy-start(f32[4096]{0:T(1024)} %param.22) | copy-start | bytes 49156
  79.7 135.3 %copy-start.6 = (f32[256]{0:T(256)S(1)}, f32[256]{0:T(256)}, u32[]{:S(2)}) copy-start(f32[256]{0:T(256)} %param.23) | copy-start | bytes 3076
  79.8 97.6 %reduce-scatter.6.cloned.1.call-start = ((), (), s32[]{:S(2)}) async-start(), calls=%async_computation.6 | async-start | bytes 147456 | tf_op jit(solution)/shard_map/reduce_scatter | solution.py:15
  137.8 39.8 %all-to-all-start.1 = ((f32[32,4,256]{2,1,0:T(4,128)}), f32[32,4,256]{2,1,0:T(4,128)S(1)}, u32[]{:S(2)}, u32[]{:S(2)}) async-start(f32[32,4,256]{2,1,0:T(4,128)} %copy.39), calls=%async_computation.2 | async-start | bytes 262144 | tf_op jit(solution)/shard_map/all_to_all | solution.py:90
  148.3 46.3 %reduce-scatter.8.cloned.1.call-start = ((), (), s32[]{:S(2)}) async-start(), calls=%async_computation.7 | async-start | bytes 24576 | tf_op jit(solution)/shard_map/reduce_scatter | solution.py:15
Sparse Core Ops, SparseCore 0:
  79.9 56.2 reduce-scatter.3
  138.9 38.3 reduce-scatter.5
  180.0 14.5 reduce-scatter.7
